TPU v7x, 128 devices: a whole 4x4x4 slice. The times are simulated.
128 devices in a mesh: fs: 16 (over z, y), tp: 8 (over x, core).
Axes of the slice: x: 4, y: 4, z: 4, core: 2. Of those that a mesh axis runs over, the one named last changes fastest.
Arguments:
- tokens: bfloat16 [16384, 2048], P(('fs', 'tp')), may hold values from -6 to 6
- first_block_norm_scale: float32 [2048], replicated, may hold values from 0.1 to 1.9
- first_block_gate_matrix: bfloat16 [2048, 5504], P('fs', 'tp'), may hold values from -0.125 to 0.125
- first_block_up_matrix: bfloat16 [2048, 5504], P('fs', 'tp'), may hold values from -0.125 to 0.125
- first_block_down_matrix: bfloat16 [5504, 2048], P('tp', 'fs'), may hold values from -0.078125 to 0.078125
- mixer_norm_scale: float32 [2048], replicated, may hold values from 0.1 to 1.9
- recurrent_input_matrix: bfloat16 [2048, 3072], P('fs', 'tp'), may hold values from -0.125 to 0.125
- output_gate_projection: bfloat16 [2048, 3072], P('fs', 'tp'), may hold values from -0.125 to 0.125
- convolution_kernel: float32 [4, 3072], P(None, 'tp'), may hold values from -2 to 2
- decay_gate_blocks: bfloat16 [16, 192, 192], P('tp'), may hold values from -0.4375 to 0.4375
- input_gate_blocks: bfloat16 [16, 192, 192], P('tp'), may hold values from -0.4375 to 0.4375
- channel_decay_weight: float32 [3072], P('tp'), may hold values from 3.5 to 11.5
- position_decay_extra: float32 [16384], P('fs'), may hold values from -0.7 to 0
- mixer_output_matrix: bfloat16 [3072, 2048], P('tp', 'fs'), may hold values from -0.109375 to 0.109375
- second_block_norm_scale: float32 [2048], replicated, may hold values from 0.1 to 1.9
- second_block_gate_matrix: bfloat16 [2048, 5504], P('fs', 'tp'), may hold values from -0.125 to 0.125
- second_block_up_matrix: bfloat16 [2048, 5504], P('fs', 'tp'), may hold values from -0.125 to 0.125
- second_block_down_matrix: bfloat16 [5504, 2048], P('tp', 'fs'), may hold values from -0.078125 to 0.078125
Outputs:
- layer_out: bfloat16 [16384, 2048], P(('fs', 'tp'))
All inputs are finite; a program needn't handle non-finite values.
Results may differ from a plain program's by a relative error of at most 0.019.
Values may be sent and summed in bfloat16 or wider, within the bound.
A program may use at most 128 MiB of HBM per device.

v0:
```python
import jax
import jax.numpy as jnp
from jax import lax
from jax.sharding import PartitionSpec as P

EPS = 1e-06
RECURRENT_WIDTH = 8.0


def in_one_piece(arrays, axis, dim, along):
    both = jnp.concatenate(arrays, axis=along)
    filled, at, gathered = (lax.all_gather(both, axis, axis=dim, tiled=True), 0, [])
    for a in arrays:
        gathered.append(lax.slice_in_dim(filled, at, at + a.shape[along], axis=along))
        at += a.shape[along]
    return tuple(gathered)


def copy_for_each(x, axis):
    copies = jnp.broadcast_to(x, (lax.axis_size(axis), *x.shape))
    return lax.all_to_all(copies, axis, split_axis=0, concat_axis=0, tiled=True)


def laid_out(tiles, dim):
    lengths = list(tiles.shape[1:])
    lengths[dim] *= tiles.shape[0]
    return jnp.moveaxis(tiles, 0, dim).reshape(lengths)


def gathered_copies(x, axis, dim):
    tiles = copy_for_each(x, axis)
    return laid_out(tiles, dim)


def cut_along(x, dim, devices):
    before, after = (x.shape[:dim], x.shape[dim + 1 :])
    return jnp.moveaxis(x.reshape(*before, devices, -1, *after), dim, 0)


def sent_and_summed(x, axis, dim):
    devices = lax.axis_size(axis)
    tiles = lax.all_to_all(cut_along(x, dim, devices), axis, 0, 0, tiled=True)
    return jnp.sum(tiles.astype(jnp.float32), axis=0)


def normed(input_token_rows, norm_scale_vector):
    values = input_token_rows.astype(jnp.float32)
    square = jnp.mean(values * values, axis=-1, keepdims=True)
    return (values * lax.rsqrt(square + EPS) * norm_scale_vector).astype(jnp.bfloat16)


def combine(earlier, later):
    decay_one, drive_one = earlier
    decay_two, drive_two = later
    return (decay_one * decay_two, decay_two * drive_one + drive_two)


def sublayer(
    residual_activations,
    norm_scale_vector,
    first_weight,
    second_weight,
    out_weight,
    middle,
    sequence,
    row_count,
):
    normal = normed(residual_activations, norm_scale_vector)
    full_first, full_second = in_one_piece((first_weight, second_weight), "fs", 0, 1)
    piece = lax.all_gather(normal, "tp", axis=0, tiled=True)
    projected = middle(
        jnp.dot(piece, full_first, preferred_element_type=jnp.float32),
        jnp.dot(piece, full_second, preferred_element_type=jnp.float32),
    )
    if sequence is not None:
        projected = sequence(projected)
    full_out = gathered_copies(out_weight, "fs", 1)
    picked = lax.slice_in_dim(projected, 0, row_count * lax.axis_size("tp"), axis=0)
    return sent_and_summed(
        jnp.dot(picked, full_out, preferred_element_type=jnp.float32).astype(jnp.bfloat16), "tp", 0
    )


def shards(
    tokens,
    first_block_norm_scale,
    first_block_gate_matrix,
    first_block_up_matrix,
    first_block_down_matrix,
    mixer_norm_scale,
    recurrent_input_matrix,
    output_gate_projection,
    convolution_kernel,
    decay_gate_blocks,
    input_gate_blocks,
    channel_decay_weight,
    position_decay_extra,
    mixer_output_matrix,
    second_block_norm_scale,
    second_block_gate_matrix,
    second_block_up_matrix,
    second_block_down_matrix,
):
    row_count = tokens.shape[0]
    residual_activations = tokens

    def feed_middle(gate_pre, up_pre):
        return (jax.nn.silu(gate_pre) * up_pre).astype(jnp.bfloat16)

    def mixer_middle(recur_pre, branch_pre):
        return jnp.concatenate(
            [recur_pre.astype(jnp.bfloat16), branch_pre.astype(jnp.bfloat16)], axis=1
        )

    def recurrent(projected):
        channels = projected.shape[1] // 2
        length = projected.shape[0]
        recur_rows = projected[:, :channels]
        branch_rows = projected[:, channels:]
        taps = convolution_kernel.shape[0]
        summed = lax.conv_general_dilated(
            recur_rows.astype(jnp.float32)[None],
            convolution_kernel[:, None, :],
            window_strides=(1,),
            padding=((taps - 1, 0),),
            dimension_numbers=("NWC", "WIO", "NWC"),
            feature_group_count=channels,
            precision=lax.Precision.HIGHEST,
        )[0]
        conv_out = summed.astype(jnp.bfloat16)
        grouped = conv_out.reshape(length, decay_gate_blocks.shape[0], decay_gate_blocks.shape[1])
        decay_gate_value = jax.nn.sigmoid(
            jnp.einsum(
                "thi,hij->thj", grouped, decay_gate_blocks, preferred_element_type=jnp.float32
            ).reshape(length, channels)
        )
        input_gate = jax.nn.sigmoid(
            jnp.einsum(
                "thi,hij->thj", grouped, input_gate_blocks, preferred_element_type=jnp.float32
            ).reshape(length, channels)
        )
        log_decay_factor = (
            -RECURRENT_WIDTH * decay_gate_value * jax.nn.softplus(-channel_decay_weight)
            + position_decay_extra[:, None]
        )
        decay_rate = jnp.exp(log_decay_factor)
        drive_in = (
            jnp.sqrt(-jnp.expm1(2.0 * log_decay_factor)) * input_gate * conv_out.astype(jnp.float32)
        )
        _, hidden_state = lax.associative_scan(combine, (decay_rate, drive_in), axis=0)
        return (
            jax.nn.gelu(branch_rows.astype(jnp.float32), approximate=True) * hidden_state
        ).astype(jnp.bfloat16)

    first_out = sublayer(
        residual_activations,
        first_block_norm_scale,
        first_block_gate_matrix,
        first_block_up_matrix,
        first_block_down_matrix,
        feed_middle,
        None,
        row_count,
    )
    residual_activations = (residual_activations.astype(jnp.float32) + 0.5 * first_out).astype(
        jnp.bfloat16
    )
    mixer_output_rows = sublayer(
        residual_activations,
        mixer_norm_scale,
        recurrent_input_matrix,
        output_gate_projection,
        mixer_output_matrix,
        mixer_middle,
        recurrent,
        row_count,
    )
    residual_activations = (residual_activations.astype(jnp.float32) + mixer_output_rows).astype(
        jnp.bfloat16
    )
    second_out = sublayer(
        residual_activations,
        second_block_norm_scale,
        second_block_gate_matrix,
        second_block_up_matrix,
        second_block_down_matrix,
        feed_middle,
        None,
        row_count,
    )
    residual_activations = (residual_activations.astype(jnp.float32) + 0.5 * second_out).astype(
        jnp.bfloat16
    )
    return residual_activations


def solution(mesh):
    in_specs = (
        P(("fs", "tp"), None),
        P(),
        P("fs", "tp"),
        P("fs", "tp"),
        P("tp", "fs"),
        P(),
        P("fs", "tp"),
        P("fs", "tp"),
        P(None, "tp"),
        P("tp", None, None),
        P("tp", None, None),
        P("tp"),
        P("fs"),
        P("tp", "fs"),
        P(),
        P("fs", "tp"),
        P("fs", "tp"),
        P("tp", "fs"),
    )
    out_specs = P(("fs", "tp"), None)
    return jax.shard_map(shards, mesh=mesh, in_specs=in_specs, out_specs=out_specs, check_vma=False)
```

profile of v0, /device:TPU:1, one launch (start us, length us, event | category | flops | bytes accessed | tf_op | source)
XLA Modules:
  0.0 540.3 jit_solution(13397318217952377570)
XLA Ops:
  7.8 2.0 fusion.40
  9.9 1.8 pad_maximum_fusion.2
  11.7 2.0 broadcast_in_dim.10
  13.7 8.7 %all-to-all-start = ((bf16[16,688,128]{2,1,0:T(8,128)(2,1)}), bf16[16,688,128]{2,1,0:T(8,128)(2,1)S(1)}, u32[]{:S(2)}, u32[]{:S(2)}) async-start(bf16[16,688,128]{2,1,0:T(8,128)(2,1)} %broadcast_in_dim.10), calls=%async_computation | async-start | bytes 5636096 | tf_op jit(solution)/shard_map/all_to_all | solution.py:21
  23.3 22.4 %all-gather.7.cloned.1.call-done = bf16[1024,2048]{1,0:T(8,128)(2,1)} async-done(((bf16[128,2048]{1,0:T(8,128)(2,1)}), bf16[1024,2048]{1,0:T(8,128)(2,1)}) %all-gather.7.cloned.1.call-update) | async-done | bytes 4194320 | tf_op jit(solution)/shard_map/all_gather | solution.py:70
  45.7 65.6 %all-gather.9.cloned.1.call-done = bf16[2048,1376]{0,1:T(8,128)(2,1)} async-done(((bf16[128,1376]{0,1:T(8,128)(2,1)}), bf16[2048,1376]{0,1:T(8,128)(2,1)}) %all-gather.9.cloned.1.call-update) | async-done | bytes 5636112 | tf_op jit(solution)/shard_map/all_gather | solution.py:12
  111.2 7.7 %fusion.10 = f32[1024,688]{0,1:T(8,128)} fusion(bf16[1024,2048]{1,0:T(8,128)(2,1)} %all-gather.7.cloned.1.call-done, bf16[2048,1376]{0,1:T(8,128)(2,1)} %all-gather.9.cloned.1.call-done), kind=kOutput, calls=%fused_computation.16 | convolution fusion | flops 2885681152 | bytes 9830400 | tf_op jit(solution)/shard_map/dot_general | solution.py:72
  118.9 11.0 %convolution_convert_fusion.2 = bf16[1024,2048]{1,0:T(8,128)(2,1)} fusion(f32[1024,688]{0,1:T(8,128)} %fusion.10, bf16[1024,2048]{1,0:T(8,128)(2,1)} %all-gather.7.cloned.1.call-done, bf16[2048,1376]{0,1:T(8,128)(2,1)} %all-gather.9.cloned.1.call-done, bf16[16,688,128]{2,1,0:T(8,128)(2,1)S(1)} %all-to-all-done), kind=kOutput, calls=%fused_computation.5 | convolution fusion | flops 5777686528 | bytes 16842752 | tf_op jit(solution)/shard_map/dot_general | solution.py:80
  130.0 54.9 %all_to_all.30 = bf16[8,128,2048]{2,1,0:T(8,128)(2,1)S(1)} all-to-all(bf16[8,128,2048]{2,1,0:T(8,128)(2,1)} %bitcast.50), channel_id=1, replica_groups=mesh['fs'=16,'tp'=8] {'tp'}, dimensions={0} | all-to-all | bytes 8388608 | tf_op jit(solution)/shard_map/all_to_all | solution.py:42
  189.6 4.7 all-to-all-start.2
  195.4 23.0 %all-gather.11.cloned.1.call-done = bf16[1024,2048]{1,0:T(8,128)(2,1)} async-done(((bf16[128,2048]{1,0:T(8,128)(2,1)}), bf16[1024,2048]{1,0:T(8,128)(2,1)}) %all-gather.11.cloned.1.call-update) | async-done | bytes 4194320 | tf_op jit(solution)/shard_map/all_gather | solution.py:70
  218.4 5.0 fusion.35
  227.1 1.7 copy.46
  229.5 1.6 copy.48
  231.1 3.4 fusion.34
  234.6 2.8 slice.256
  237.4 2.8 slice.257
  240.2 2.8 slice.255
  242.9 2.8 slice.259
  245.7 3.2 fusion.89
  248.8 3.0 slice.262
  251.9 3.1 slice.263
  254.9 3.1 slice.261
  258.0 3.1 slice.265
  261.1 2.3 fusion.90
  263.4 1.7 slice.268
  265.1 1.7 slice.269
  266.8 1.7 slice.267
  268.5 1.7 slice.271
  274.1 1.7 fusion.92
  275.9 1.5 slice.280
  281.9 1.5 fusion.93
  316.9 1.5 slice.278
  324.3 1.7 slice.323
  327.3 3.1 slice.260
  330.4 3.1 slice.325
  334.8 2.8 slice.327
  337.6 2.8 slice.254
  346.6 3.1 pad.80
  351.3 10.3 %convolution_convert_fusion = bf16[1024,2048]{1,0:T(8,128)(2,1)} fusion(bf16[384,2048]{0,1:T(8,128)(2,1)} %bitcast.12, f32[1024,384]{1,0:T(8,128)S(1)} %pad.79, f32[1024,384]{1,0:T(8,128)} %pad.80, bf16[1024,2048]{1,0:T(8,128)(2,1)} %all-gather.11.cloned.1.call-done, bf16[2048,768]{1,0:T(8,128)(2,1)} %all-gather.13.cloned.1.call-done), kind=kOutput, calls=%fused_computation.3 | convolution fusion | flops 3228434432 | bytes 14680064 | tf_op jit(solution)/shard_map/dot_general | solution.py:80
  361.6 52.5 %all_to_all.31 = bf16[8,128,2048]{2,1,0:T(8,128)(2,1)S(1)} all-to-all(bf16[8,128,2048]{2,1,0:T(8,128)(2,1)} %bitcast.49), channel_id=1, replica_groups=mesh['fs'=16,'tp'=8] {'tp'}, dimensions={0} | all-to-all | bytes 8388608 | tf_op jit(solution)/shard_map/all_to_all | solution.py:42
  416.5 2.0 broadcast_in_dim.27
  418.5 6.7 %all-to-all-start.4 = ((bf16[16,688,128]{2,1,0:T(8,128)(2,1)}), bf16[16,688,128]{2,1,0:T(8,128)(2,1)S(1)}, u32[]{:S(2)}, u32[]{:S(2)}) async-start(bf16[16,688,128]{2,1,0:T(8,128)(2,1)} %broadcast_in_dim.27), calls=%async_computation.4 | async-start | bytes 5636096 | tf_op jit(solution)/shard_map/all_to_all | solution.py:21
  425.3 23.6 %all-gather.15.cloned.1.call-done = bf16[1024,2048]{1,0:T(8,128)(2,1)} async-done(((bf16[128,2048]{1,0:T(8,128)(2,1)}), bf16[1024,2048]{1,0:T(8,128)(2,1)}) %all-gather.15.cloned.1.call-update) | async-done | bytes 4194320 | tf_op jit(solution)/shard_map/all_gather | solution.py:70
  448.9 7.7 %fusion.6 = f32[1024,688]{0,1:T(8,128)} fusion(bf16[1024,2048]{1,0:T(8,128)(2,1)} %all-gather.15.cloned.1.call-done, bf16[2048,1376]{0,1:T(8,128)(2,1)} %all-gather.17.cloned.1.call-done), kind=kOutput, calls=%fused_computation.12 | convolution fusion | flops 2885681152 | bytes 9830400 | tf_op jit(solution)/shard_map/dot_general | solution.py:72
  456.6 9.6 %all-to-all-done.4 = bf16[16,688,128]{2,1,0:T(8,128)(2,1)S(1)} async-done(((bf16[16,688,128]{2,1,0:T(8,128)(2,1)}), bf16[16,688,128]{2,1,0:T(8,128)(2,1)S(1)}, u32[]{:S(2)}, u32[]{:S(2)}) %all-to-all-start.4) | async-done | bytes 2818080 | tf_op jit(solution)/shard_map/all_to_all | solution.py:21
  466.2 11.0 %convolution_convert_fusion.1 = bf16[1024,2048]{1,0:T(8,128)(2,1)} fusion(f32[1024,688]{0,1:T(8,128)} %fusion.6, bf16[1024,2048]{1,0:T(8,128)(2,1)} %all-gather.15.cloned.1.call-done, bf16[2048,1376]{0,1:T(8,128)(2,1)} %all-gather.17.cloned.1.call-done, bf16[16,688,128]{2,1,0:T(8,128)(2,1)S(1)} %all-to-all-done.4), kind=kOutput, calls=%fused_computation.4 | convolution fusion | flops 5777686528 | bytes 16842752 | tf_op jit(solution)/shard_map/dot_general | solution.py:80
  477.3 54.5 %all_to_all.32 = bf16[8,128,2048]{2,1,0:T(8,128)(2,1)S(1)} all-to-all(bf16[8,128,2048]{2,1,0:T(8,128)(2,1)} %bitcast.51), channel_id=1, replica_groups=mesh['fs'=16,'tp'=8] {'tp'}, dimensions={0} | all-to-all | bytes 8388608 | tf_op jit(solution)/shard_map/all_to_all | solution.py:42
  (213 shorter events, 73.6 us)
Async XLA Ops:
  6.5 219.9 %copy-start = (bf16[2,192,192]{2,1,0:T(8,128)(2,1)S(1)}, bf16[2,192,192]{2,1,0:T(8,128)(2,1)}, u32[]{:S(2)}) copy-start(bf16[2,192,192]{2,1,0:T(8,128)(2,1)} %param.27) | copy-start | bytes 442372
  6.5 5.2 copy-start.10
  6.5 39.1 %all-gather.7.cloned.1.call-start = ((), (), s32[]{:S(2)}) async-start(), calls=%async_computation.6 | async-start | bytes 4718592 | tf_op jit(solution)/shard_map/all_gather | solution.py:70
  9.9 101.4 %all-gather.9.cloned.1.call-start = ((), (), s32[]{:S(2)}) async-start(), calls=%async_computation.7 | async-start | bytes 5988352 | tf_op jit(solution)/shard_map/all_gather | solution.py:12
  13.7 8.8 %copy-start.15 = (bf16[128,384]{1,0:T(8,128)(2,1)S(1)}, bf16[128,384]{1,0:T(8,128)(2,1)}, u32[]{:S(2)}) copy-start(bf16[128,384]{1,0:T(8,128)(2,1)} %param.25) | copy-start | bytes 294916
  13.7 8.8 %copy-start.16 = (bf16[128,384]{1,0:T(8,128)(2,1)S(1)}, bf16[128,384]{1,0:T(8,128)(2,1)}, u32[]{:S(2)}) copy-start(bf16[128,384]{1,0:T(8,128)(2,1)} %param.24) | copy-start | bytes 294916
  13.7 105.2 %all-to-all-start = ((bf16[16,688,128]{2,1,0:T(8,128)(2,1)}), bf16[16,688,128]{2,1,0:T(8,128)(2,1)S(1)}, u32[]{:S(2)}, u32[]{:S(2)}) async-start(bf16[16,688,128]{2,1,0:T(8,128)(2,1)} %broadcast_in_dim.10), calls=%async_computation | async-start | bytes 5636096 | tf_op jit(solution)/shard_map/all_to_all | solution.py:21
  22.5 172.9 %all-gather.13.cloned.1.call-start = ((), (), s32[]{:S(2)}) async-start(), calls=%async_computation.9 | async-start | bytes 3342336 | tf_op jit(solution)/shard_map/all_gather | solution.py:12
  23.2 195.2 %all-gather.11.cloned.1.call-start = ((), (), s32[]{:S(2)}) async-start(), calls=%async_computation.8 | async-start | bytes 4718592 | tf_op jit(solution)/shard_map/all_gather | solution.py:70
  184.9 1.0 copy-start.3
  184.9 2.1 copy-start.25
  186.0 2.1 copy-start.14
  186.2 0.8 copy-start.4
  188.0 6.3 %copy-start.11 = (bf16[128,688]{0,1:T(8,128)(2,1)S(1)}, bf16[128,688]{0,1:T(8,128)(2,1)}, u32[]{:S(2)}) copy-start(bf16[128,688]{0,1:T(8,128)(2,1)} %param.34) | copy-start | bytes 528388
  188.0 6.3 %copy-start.12 = (bf16[128,688]{0,1:T(8,128)(2,1)S(1)}, bf16[128,688]{0,1:T(8,128)(2,1)}, u32[]{:S(2)}) copy-start(bf16[128,688]{0,1:T(8,128)(2,1)} %param.33) | copy-start | bytes 528388
  188.2 7.1 %copy-start.35 = (f32[384]{0:T(512)S(1)}, f32[384]{0:T(512)}, u32[]{:S(2)}) copy-start(f32[384]{0:T(512)} %param.29) | copy-start | bytes 4612
  189.6 161.7 %all-to-all-start.2 = ((bf16[16,384,128]{1,2,0:T(8,128)(2,1)}), bf16[16,384,128]{1,2,0:T(8,128)(2,1)}, u32[]{:S(2)}, u32[]{:S(2)}) async-start(bf16[16,384,128]{1,2,0:T(8,128)(2,1)} %broadcast_in_dim.26), calls=%async_computation.2 | async-start | bytes 3145728 | tf_op jit(solution)/shard_map/all_to_all | solution.py:21
  194.3 231.0 %all-gather.17.cloned.1.call-start = ((), (), s32[]{:S(2)}) async-start(), calls=%async_computation.11 | async-start | bytes 5988352 | tf_op jit(solution)/shard_map/all_gather | solution.py:12
  195.1 253.8 %all-gather.15.cloned.1.call-start = ((), (), s32[]{:S(2)}) async-start(), calls=%async_computation.10 | async-start | bytes 4718592 | tf_op jit(solution)/shard_map/all_gather | solution.py:70
  223.4 0.7 copy-start.37
  223.4 0.7 copy-start.38
  226.1 1.1 copy-start.2
  227.1 1.7 copy-start.36
  229.5 1.6 copy-start.34
  323.1 17.9 %copy-start.23 = (f32[2,384]{1,0:T(2,128)S(1)}, f32[2,384]{1,0:T(2,128)}, u32[]{:S(2)}) copy-start(f32[2,384]{1,0:T(2,128)} %slice.304) | copy-start | bytes 9220
  323.1 17.9 %copy-start.24 = (f32[2,384]{1,0:T(2,128)S(1)}, f32[2,384]{1,0:T(2,128)}, u32[]{:S(2)}) copy-start(f32[2,384]{1,0:T(2,128)} %slice.305) | copy-start | bytes 9220
  323.1 17.9 %copy-start.27 = (f32[2,384]{1,0:T(2,128)S(1)}, f32[2,384]{1,0:T(2,128)}, u32[]{:S(2)}) copy-start(f32[2,384]{1,0:T(2,128)} %slice.307) | copy-start | bytes 9220
  323.1 18.0 %copy-start.20 = (f32[4,384]{1,0:T(4,128)S(1)}, f32[4,384]{1,0:T(4,128)}, u32[]{:S(2)}) copy-start(f32[4,384]{1,0:T(4,128)} %get-tuple-element.28) | copy-start | bytes 18436
  323.1 18.7 %copy-start.21 = (f32[3,384]{1,0:T(4,128)S(1)}, f32[3,384]{1,0:T(4,128)}, u32[]{:S(2)}) copy-start(f32[3,384]{1,0:T(4,128)} %slice.296) | copy-start | bytes 13828
  323.1 18.7 %copy-start.22 = (f32[3,384]{1,0:T(4,128)S(1)}, f32[3,384]{1,0:T(4,128)}, u32[]{:S(2)}) copy-start(f32[3,384]{1,0:T(4,128)} %slice.313) | copy-start | bytes 13828
  323.1 18.7 %copy-start.32 = (f32[1,384]{1,0:T(1,128)S(1)}, f32[1,384]{1,0:T(1,128)}, u32[]{:S(2)}) copy-start(f32[1,384]{1,0:T(1,128)} %slice.345) | copy-start | bytes 4612
  323.1 18.8 %copy-start.19 = (f32[7,384]{1,0:T(8,128)S(1)}, f32[7,384]{1,0:T(8,128)}, u32[]{:S(2)}) copy-start(f32[7,384]{1,0:T(8,128)} %slice.315) | copy-start | bytes 32260
  323.2 18.8 %copy-start.31 = (f32[1,384]{1,0:T(1,128)S(1)}, f32[1,384]{1,0:T(1,128)}, u32[]{:S(2)}) copy-start(f32[1,384]{1,0:T(1,128)} %slice.344) | copy-start | bytes 4612
  324.3 17.7 %copy-start.17 = (f32[15,384]{1,0:T(8,128)S(1)}, f32[15,384]{1,0:T(8,128)}, u32[]{:S(2)}) copy-start(f32[15,384]{1,0:T(8,128)} %slice.284) | copy-start | bytes 69124
  324.3 17.7 %copy-start.18 = (f32[15,384]{1,0:T(8,128)S(1)}, f32[15,384]{1,0:T(8,128)}, u32[]{:S(2)}) copy-start(f32[15,384]{1,0:T(8,128)} %slice.317) | copy-start | bytes 69124
  324.3 17.8 %copy-start.30 = (f32[1,384]{1,0:T(1,128)S(1)}, f32[1,384]{1,0:T(1,128)}, u32[]{:S(2)}) copy-start(f32[1,384]{1,0:T(1,128)} %slice.343) | copy-start | bytes 4612
  340.4 5.2 copy-start.9
  340.4 5.3 copy-start.29
  343.7 2.1 copy-start.7
  343.7 2.1 copy-start.8
  345.5 0.7 copy-start.33
  346.3 3.4 copy-start.6
  346.6 4.4 copy-start.28
  414.2 1.0 copy-start.5
  414.2 1.3 copy-start.26
  415.2 1.3 copy-start.13
  418.5 47.7 %all-to-all-start.4 = ((bf16[16,688,128]{2,1,0:T(8,128)(2,1)}), bf16[16,688,128]{2,1,0:T(8,128)(2,1)S(1)}, u32[]{:S(2)}, u32[]{:S(2)}) async-start(bf16[16,688,128]{2,1,0:T(8,128)(2,1)} %broadcast_in_dim.27), calls=%async_computation.4 | async-start | bytes 5636096 | tf_op jit(solution)/shard_map/all_to_all | solution.py:21
  477.3 56.2 %copy-start.1 = (bf16[2,192,192]{2,1,0:T(8,128)(2,1)S(1)}, bf16[2,192,192]{2,1,0:T(8,128)(2,1)}, u32[]{:S(2)}) copy-start(bf16[2,192,192]{2,1,0:T(8,128)(2,1)} %param.27) | copy-start | bytes 442372
Sparse Core Ops, SparseCore 0:
  10.0 35.6 all-gather.6
  47.8 63.4 all-gather.8
  113.4 47.9 all-gather.12
  188.2 30.1 all-gather.10
  220.4 62.0 all-gather.16
  416.6 32.2 all-gather.14
where the time goes:
time: 544 us; the launch traced here: 540 us
  blocking collectives  162 us (30%)
  waiting for transfers between devices  144 us (26%)
  local copies, waits for them, and re-layouts  108 us (20%)
  matrix products  55.6 us (10%)
  other arithmetic  35.3 us (6%)
  starting transfers between devices  20.5 us (4%)
  between operations  14.4 us (3%)
    all_to_all x3, blocking collectives, sent_and_summed(): tiles = lax.all_to_all(cut_along(x, dim, devices), axis, 0, 0, tiled=True)  162 us
    slice x60, local copies, waits for them, and re-layouts, recurrent(): lax.associative_scan(combine, (decay_rate, drive_in), axis=0)  92.2 us
    all_gather x3, waiting for transfers between devices, sublayer(): piece = lax.all_gather(normal, 'tp', axis=0, tiled=True)  69 us
    all_gather x3, waiting for transfers between devices, in_one_piece(): lax.all_gather(both, axis, axis=dim, tiled=True)  65.6 us
    dot_general x3, matrix products, sublayer(): jnp.dot(picked, full_out, preferred_element_type=jnp.float32)  32.4 us
    dot_general x3, matrix products, sublayer(): jnp.dot(piece, full_first, preferred_element_type=jnp.float32)  20.4 us
    all_to_all x3, starting transfers between devices, copy_for_each(): return lax.all_to_all(copies, axis, split_axis=0, concat_axis=0, tiled=True)  20.1 us
    mul x8, other arithmetic, combine(): return (decay_one * decay_two, decay_two * drive_one + drive_two)  14.1 us
  transfers between devices with their start and end apart: 9, of which 5 were waited for; matrix products, arithmetic and copies ran while one was open for 34% of the time, Pallas kernels for 0%

commit v1 on v0

--- a/solution.py
+++ b/solution.py
@@ -5,6 +5,27 @@
 
 EPS = 1e-06
 RECURRENT_WIDTH = 8.0
+
+
+def gather_around(shard, axis, dim):
+    length, position, rows = (lax.axis_size(axis), lax.axis_index(axis), shard.shape[dim])
+    forward = [(i, (i + 1) % length) for i in range(length)]
+    left = [(i, (i - 1) % length) for i in range(length)]
+    result = jnp.zeros((*shard.shape[:dim], length * rows, *shard.shape[dim + 1 :]), shard.dtype)
+    result = lax.dynamic_update_slice_in_dim(result, shard, position * rows, axis=dim)
+    from_left = from_right = shard
+    half = length // 2
+    for step in range(1, half + 1):
+        from_left = lax.ppermute(from_left, axis, forward)
+        result = lax.dynamic_update_slice_in_dim(
+            result, from_left, (position - step) % length * rows, axis=dim
+        )
+        if step < length - half:
+            from_right = lax.ppermute(from_right, axis, left)
+            result = lax.dynamic_update_slice_in_dim(
+                result, from_right, (position + step) % length * rows, axis=dim
+            )
+    return result
 
 
 def in_one_piece(arrays, axis, dim, along):
@@ -67,7 +88,7 @@
 ):
     normal = normed(residual_activations, norm_scale_vector)
     full_first, full_second = in_one_piece((first_weight, second_weight), "fs", 0, 1)
-    piece = lax.all_gather(normal, "tp", axis=0, tiled=True)
+    piece = gather_around(normal, "tp", 0)
     projected = middle(
         jnp.dot(piece, full_first, preferred_element_type=jnp.float32),
         jnp.dot(piece, full_second, preferred_element_type=jnp.float32),

time: 544 us -> 576 us (1.059)
  waiting for transfers between devices: 144 us -> 101 us
  local copies, waits for them, and re-layouts: 108 us -> 145 us
  starting transfers between devices: 20.5 us -> 42.9 us
  other arithmetic: 35.3 us -> 45.4 us
    all_gather x3 -> x0, waiting for transfers between devices: 69 us -> none  [sublayer(): piece = lax.all_gather(normal, 'tp', axis=0, tiled=True)]
    ppermute x0 -> x21, waiting for transfers between devices: none -> 41.1 us  [the longest x9 22 us: gather_around(): from_right = lax.ppermute(from_right, axis, left)]
    dynamic_update_slice x0 -> x21, local copies, waits for them, and re-layouts: none -> 25.1 us  [the longest x12 14.3 us: gather_around(): lax.dynamic_update_slice_in_dim(result, from_left, (position - step) % le...]
    ppermute x0 -> x21, starting transfers between devices: none -> 24 us  [the longest x12 18.6 us: gather_around(): from_left = lax.ppermute(from_left, axis, forward)]
    all_gather x3, waiting for transfers between devices: 65.6 us -> 45.5 us  [in_one_piece(): lax.all_gather(both, axis, axis=dim, tiled=True)]
    dot_general x0 -> x2, matrix products: none -> 15.4 us  [sublayer(): jnp.dot(piece, full_second, preferred_element_type=jnp.float32)]
    dot_general x3 -> x1, matrix products: 20.4 us -> 5.09 us  [sublayer(): jnp.dot(piece, full_first, preferred_element_type=jnp.float32)]
    pad x18, local copies, waits for them, and re-layouts: 3.85 us -> 10.2 us  [recurrent(): lax.associative_scan(combine, (decay_rate, drive_in), axis=0)]
  transfers between devices with their start and end apart: 9 -> 27, of which waited for: 5 -> 11; matrix products, arithmetic and copies ran while one was open for 34% -> 40% of each run, Pallas kernels for 0% -> 0%
where the time goes in v1:
time: 576 us; the launch traced here: 571 us
  blocking collectives  167 us (29%)
  local copies, waits for them, and re-layouts  145 us (25%)
  waiting for transfers between devices  101 us (18%)
  matrix products  56.2 us (10%)
  other arithmetic  45.4 us (8%)
  starting transfers between devices  42.9 us (7%)
  between operations  13.9 us (2%)
    all_to_all x3, blocking collectives, sent_and_summed(): tiles = lax.all_to_all(cut_along(x, dim, devices), axis, 0, 0, tiled=True)  167 us
    slice x60, local copies, waits for them, and re-layouts, recurrent(): lax.associative_scan(combine, (decay_rate, drive_in), axis=0)  90.3 us
    all_gather x3, waiting for transfers between devices, in_one_piece(): lax.all_gather(both, axis, axis=dim, tiled=True)  45.5 us
    dot_general x3, matrix products, sublayer(): jnp.dot(picked, full_out, preferred_element_type=jnp.float32)  32.9 us
    ppermute x9, waiting for transfers between devices, gather_around(): from_right = lax.ppermute(from_right, axis, left)  22 us
    ppermute x12, waiting for transfers between devices, gather_around(): from_left = lax.ppermute(from_left, axis, forward)  19 us
    ppermute x12, starting transfers between devices, gather_around(): from_left = lax.ppermute(from_left, axis, forward)  18.6 us
    all_to_all x3, starting transfers between devices, copy_for_each(): return lax.all_to_all(copies, axis, split_axis=0, concat_axis=0, tiled=True)  18.6 us
  transfers between devices with their start and end apart: 27, of which 11 were waited for; matrix products, arithmetic and copies ran while one was open for 40% of the time, Pallas kernels for 0%

profile of v1, /device:TPU:1, one launch (start us, length us, event | category | flops | bytes accessed | tf_op | source)
XLA Modules:
  0.0 571.4 jit_solution(10298296681874629518)
XLA Ops:
  9.7 2.6 broadcast.120.clone.1
  13.5 2.6 collective-permute-start
  16.1 6.4 %collective-permute-done = bf16[128,2048]{1,0:T(8,128)(2,1)} collective-permute-done((bf16[128,2048]{1,0:T(8,128)(2,1)}, bf16[128,2048]{1,0:T(8,128)(2,1)}, u32[]{:S(2)}, u32[]{:S(2)}) %collective-permute-start) | collective-permute-done | bytes 524320 | tf_op jit(solution)/shard_map/ppermute | solution.py:19
  22.5 2.5 collective-permute-start.2
  25.0 2.0 broadcast_in_dim.10
  26.9 7.8 %all-to-all-start = ((bf16[16,688,128]{2,1,0:T(8,128)(2,1)}), bf16[16,688,128]{2,1,0:T(8,128)(2,1)S(1)}, u32[]{:S(2)}, u32[]{:S(2)}) async-start(bf16[16,688,128]{2,1,0:T(8,128)(2,1)} %broadcast_in_dim.10), calls=%async_computation | async-start | bytes 5636096 | tf_op jit(solution)/shard_map/all_to_all | solution.py:42
  50.3 2.7 collective-permute-done.5
  54.7 45.5 %all-gather.4.cloned.1.call-done = bf16[2048,1376]{0,1:T(8,128)(2,1)} async-done(((bf16[128,1376]{0,1:T(8,128)(2,1)}), bf16[2048,1376]{0,1:T(8,128)(2,1)}) %all-gather.4.cloned.1.call-update) | async-done | bytes 5636112 | tf_op jit(solution)/shard_map/all_gather | solution.py:33
  100.2 7.7 %fusion.8 = f32[1024,688]{0,1:T(8,128)} fusion(bf16[1024,2048]{1,0:T(8,128)(2,1)} %constant_dynamic-update-slice_fusion.16, bf16[2048,1376]{0,1:T(8,128)(2,1)} %all-gather.4.cloned.1.call-done), kind=kOutput, calls=%fused_computation.14 | convolution fusion | flops 2885681152 | bytes 9830400 | tf_op jit(solution)/shard_map/dot_general | solution.py:94
  107.9 11.3 %convolution_convert_fusion.2 = bf16[1024,2048]{1,0:T(8,128)(2,1)} fusion(f32[1024,688]{0,1:T(8,128)} %fusion.8, bf16[1024,2048]{1,0:T(8,128)(2,1)} %constant_dynamic-update-slice_fusion.16, bf16[2048,1376]{0,1:T(8,128)(2,1)} %all-gather.4.cloned.1.call-done, bf16[16,688,128]{2,1,0:T(8,128)(2,1)S(1)} %all-to-all-done), kind=kOutput, calls=%fused_computation.5 | convolution fusion | flops 5777686528 | bytes 16842752 | tf_op jit(solution)/shard_map/dot_general | solution.py:101
  119.2 55.2 %all_to_all.30 = bf16[8,128,2048]{2,1,0:T(8,128)(2,1)S(1)} all-to-all(bf16[8,128,2048]{2,1,0:T(8,128)(2,1)} %bitcast.50), channel_id=1, replica_groups=mesh['fs'=16,'tp'=8] {'tp'}, dimensions={0} | all-to-all | bytes 8388608 | tf_op jit(solution)/shard_map/all_to_all | solution.py:63
  176.4 2.0 copy-done.6
  180.2 6.1 %collective-permute-done.7 = bf16[128,2048]{1,0:T(8,128)(2,1)S(1)} collective-permute-done((bf16[128,2048]{1,0:T(8,128)(2,1)S(1)}, bf16[128,2048]{1,0:T(8,128)(2,1)S(1)}, u32[]{:S(2)}, u32[]{:S(2)}) %collective-permute-start.7) | collective-permute-done | bytes 524320 | tf_op jit(solution)/shard_map/ppermute | solution.py:19
  186.4 2.5 collective-permute-start.9
  190.3 4.4 all-to-all-start.2
  199.2 5.6 collective-permute-done.10
  209.1 4.7 collective-permute-done.12
  215.6 5.1 fusion.41
  228.4 3.4 fusion.32
  231.8 2.8 slice.256
  234.6 2.8 slice.257
  237.3 2.7 slice.255
  240.1 2.8 slice.259
  242.9 3.2 fusion.94
  246.0 3.1 slice.262
  249.1 3.1 slice.263
  252.2 3.1 slice.261
  255.2 3.1 slice.265
  258.3 2.4 fusion.95
  325.8 1.9 pad.68
  342.4 3.1 slice.260
  345.5 3.1 slice.325
  349.9 2.8 slice.254
  352.7 2.8 slice.327
  358.7 3.1 pad.80
  363.4 10.3 %convolution_convert_fusion = bf16[1024,2048]{1,0:T(8,128)(2,1)} fusion(bf16[384,2048]{0,1:T(8,128)(2,1)} %bitcast.12, f32[1024,384]{1,0:T(8,128)S(1)} %pad.79, f32[1024,384]{1,0:T(8,128)} %pad.80, bf16[1024,2048]{1,0:T(8,128)(2,1)} %constant_dynamic-update-slice_fusion.8, bf16[2048,768]{1,0:T(8,128)(2,1)} %all-gather.6.cloned.1.call-done), kind=kOutput, calls=%fused_computation.3 | convolution fusion | flops 3228434432 | bytes 14680064 | tf_op jit(solution)/shard_map/dot_general | solution.py:101
  373.7 57.9 %all_to_all.31 = bf16[8,128,2048]{2,1,0:T(8,128)(2,1)S(1)} all-to-all(bf16[8,128,2048]{2,1,0:T(8,128)(2,1)} %bitcast.49), channel_id=1, replica_groups=mesh['fs'=16,'tp'=8] {'tp'}, dimensions={0} | all-to-all | bytes 8388608 | tf_op jit(solution)/shard_map/all_to_all | solution.py:63
  432.9 2.6 broadcast.120
  438.4 6.4 %collective-permute-done.14 = bf16[128,2048]{1,0:T(8,128)(2,1)} collective-permute-done((bf16[128,2048]{1,0:T(8,128)(2,1)}, bf16[128,2048]{1,0:T(8,128)(2,1)}, u32[]{:S(2)}, u32[]{:S(2)}) %collective-permute-start.14) | collective-permute-done | bytes 524320 | tf_op jit(solution)/shard_map/ppermute | solution.py:19
  444.8 2.5 collective-permute-start.16
  447.3 2.0 broadcast_in_dim.27
  449.3 6.4 %all-to-all-start.4 = ((bf16[16,688,128]{2,1,0:T(8,128)(2,1)}), bf16[16,688,128]{2,1,0:T(8,128)(2,1)S(1)}, u32[]{:S(2)}, u32[]{:S(2)}) async-start(bf16[16,688,128]{2,1,0:T(8,128)(2,1)} %broadcast_in_dim.27), calls=%async_computation.4 | async-start | bytes 5636096 | tf_op jit(solution)/shard_map/all_to_all | solution.py:42
  461.2 3.6 collective-permute-done.17
  470.1 3.6 collective-permute-done.19
  475.4 7.7 %fusion.4 = f32[1024,688]{0,1:T(8,128)} fusion(bf16[1024,2048]{1,0:T(8,128)(2,1)} %constant_dynamic-update-slice_fusion, bf16[2048,1376]{0,1:T(8,128)(2,1)} %all-gather.8.cloned.1.call-done), kind=kOutput, calls=%fused_computation.10 | convolution fusion | flops 2885681152 | bytes 9830400 | tf_op jit(solution)/shard_map/dot_general | solution.py:94
  483.1 14.8 %all-to-all-done.4 = bf16[16,688,128]{2,1,0:T(8,128)(2,1)S(1)} async-done(((bf16[16,688,128]{2,1,0:T(8,128)(2,1)}), bf16[16,688,128]{2,1,0:T(8,128)(2,1)S(1)}, u32[]{:S(2)}, u32[]{:S(2)}) %all-to-all-start.4) | async-done | bytes 2818080 | tf_op jit(solution)/shard_map/all_to_all | solution.py:42
  497.9 11.3 %convolution_convert_fusion.1 = bf16[1024,2048]{1,0:T(8,128)(2,1)} fusion(f32[1024,688]{0,1:T(8,128)} %fusion.4, bf16[1024,2048]{1,0:T(8,128)(2,1)} %constant_dynamic-update-slice_fusion, bf16[2048,1376]{0,1:T(8,128)(2,1)} %all-gather.8.cloned.1.call-done, bf16[16,688,128]{2,1,0:T(8,128)(2,1)S(1)} %all-to-all-done.4), kind=kOutput, calls=%fused_computation.4 | convolution fusion | flops 5777686528 | bytes 16842752 | tf_op jit(solution)/shard_map/dot_general | solution.py:101
  509.2 54.0 %all_to_all.32 = bf16[8,128,2048]{2,1,0:T(8,128)(2,1)S(1)} all-to-all(bf16[8,128,2048]{2,1,0:T(8,128)(2,1)} %bitcast.51), channel_id=1, replica_groups=mesh['fs'=16,'tp'=8] {'tp'}, dimensions={0} | all-to-all | bytes 8388608 | tf_op jit(solution)/shard_map/all_to_all | solution.py:63
  (246 shorter events, 148.6 us)
Async XLA Ops:
  6.5 217.2 %copy-start = (bf16[2,192,192]{2,1,0:T(8,128)(2,1)S(1)}, bf16[2,192,192]{2,1,0:T(8,128)(2,1)}, u32[]{:S(2)}) copy-start(bf16[2,192,192]{2,1,0:T(8,128)(2,1)} %param.27) | copy-start | bytes 442372
  6.5 5.8 %copy-start.5 = (bf16[128,2048]{1,0:T(8,128)(2,1)S(1)}, bf16[128,2048]{1,0:T(8,128)(2,1)}, u32[]{:S(2)}) copy-start(bf16[128,2048]{1,0:T(8,128)(2,1)} %param.18) | copy-start | bytes 1572868
  6.5 5.8 %copy-start.18 = (f32[2048]{0:T(1024)S(1)}, f32[2048]{0:T(1024)}, u32[]{:S(2)}) copy-start(f32[2048]{0:T(1024)} %param.19) | copy-start | bytes 24580
  6.5 93.7 %all-gather.4.cloned.1.call-start = ((), (), s32[]{:S(2)}) async-start(), calls=%async_computation.6 | async-start | bytes 5988352 | tf_op jit(solution)/shard_map/all_gather | solution.py:33
  8.4 16.6 %copy-start.11 = (bf16[688,128]{1,0:T(8,128)(2,1)S(1)}, bf16[688,128]{1,0:T(8,128)(2,1)}, u32[]{:S(2)}) copy-start(bf16[688,128]{1,0:T(8,128)(2,1)} %param.22) | copy-start | bytes 528388
  13.5 9.0 %collective-permute-start = (bf16[128,2048]{1,0:T(8,128)(2,1)}, bf16[128,2048]{1,0:T(8,128)(2,1)}, u32[]{:S(2)}, u32[]{:S(2)}) collective-permute-start(bf16[128,2048]{1,0:T(8,128)(2,1)} %get-tuple-element.14), channel_id=1, source_target_pairs={{0,1},{1,2},{2,3},{3,4},{4,5},{5,6},{6,7},{7,0},{8,9},{9,10},{10,1... | collective-permute-start | bytes 1572872 | tf_op jit(solution)/shard_map/ppermute | solution.py:19
  16.0 18.7 %collective-permute-start.1 = (bf16[128,2048]{1,0:T(8,128)(2,1)}, bf16[128,2048]{1,0:T(8,128)(2,1)}, u32[]{:S(2)}, u32[]{:S(2)}) collective-permute-start(bf16[128,2048]{1,0:T(8,128)(2,1)} %get-tuple-element.14), channel_id=1, source_target_pairs={{0,7},{1,0},{2,1},{3,2},{4,3},{5,4},{6,5},{7,6},{8,15},{9,8},{10,9... | collective-permute-start | bytes 1572872 | tf_op jit(solution)/shard_map/ppermute | solution.py:24
  22.5 14.5 %collective-permute-start.2 = (bf16[128,2048]{1,0:T(8,128)(2,1)}, bf16[128,2048]{1,0:T(8,128)(2,1)}, u32[]{:S(2)}, u32[]{:S(2)}) collective-permute-start(bf16[128,2048]{1,0:T(8,128)(2,1)} %collective-permute-done), channel_id=1, source_target_pairs={{0,1},{1,2},{2,3},{3,4},{4,5},{5,6},{6,7},{7,0},{8,9},{9,10},{10,1... | collective-permute-start | bytes 1572872 | tf_op jit(solution)/shard_map/ppermute | solution.py:19
  26.9 81.0 %all-to-all-start = ((bf16[16,688,128]{2,1,0:T(8,128)(2,1)}), bf16[16,688,128]{2,1,0:T(8,128)(2,1)S(1)}, u32[]{:S(2)}, u32[]{:S(2)}) async-start(bf16[16,688,128]{2,1,0:T(8,128)(2,1)} %broadcast_in_dim.10), calls=%async_computation | async-start | bytes 5636096 | tf_op jit(solution)/shard_map/all_to_all | solution.py:42
  34.7 180.9 %all-gather.6.cloned.1.call-start = ((), (), s32[]{:S(2)}) async-start(), calls=%async_computation.7 | async-start | bytes 3342336 | tf_op jit(solution)/shard_map/all_gather | solution.py:33
  34.8 9.1 %collective-permute-start.3 = (bf16[128,2048]{1,0:T(8,128)(2,1)}, bf16[128,2048]{1,0:T(8,128)(2,1)}, u32[]{:S(2)}, u32[]{:S(2)}) collective-permute-start(bf16[128,2048]{1,0:T(8,128)(2,1)} %collective-permute-done.1), channel_id=1, source_target_pairs={{0,7},{1,0},{2,1},{3,2},{4,3},{5,4},{6,5},{7,6},{8,15},{9,8},{10,9... | collective-permute-start | bytes 1572872 | tf_op jit(solution)/shard_map/ppermute | solution.py:24
  37.0 9.8 %collective-permute-start.4 = (bf16[128,2048]{1,0:T(8,128)(2,1)}, bf16[128,2048]{1,0:T(8,128)(2,1)S(1)}, u32[]{:S(2)}, u32[]{:S(2)}) collective-permute-start(bf16[128,2048]{1,0:T(8,128)(2,1)} %collective-permute-done.2), channel_id=1, source_target_pairs={{0,1},{1,2},{2,3},{3,4},{4,5},{5,6},{6,7},{7,0},{8,9},{9,10},{10,1... | collective-permute-start | bytes 1572872 | tf_op jit(solution)/shard_map/ppermute | solution.py:19
  43.9 9.1 %collective-permute-start.5 = (bf16[128,2048]{1,0:T(8,128)(2,1)}, bf16[128,2048]{1,0:T(8,128)(2,1)S(1)}, u32[]{:S(2)}, u32[]{:S(2)}) collective-permute-start(bf16[128,2048]{1,0:T(8,128)(2,1)} %collective-permute-done.3), channel_id=1, source_target_pairs={{0,7},{1,0},{2,1},{3,2},{4,3},{5,4},{6,5},{7,6},{8,15},{9,8},{10,9... | collective-permute-start | bytes 1572872 | tf_op jit(solution)/shard_map/ppermute | solution.py:24
  46.8 7.1 %collective-permute-start.6 = (bf16[128,2048]{1,0:T(8,128)(2,1)S(1)}, bf16[128,2048]{1,0:T(8,128)(2,1)S(1)}, u32[]{:S(2)}, u32[]{:S(2)}) collective-permute-start(bf16[128,2048]{1,0:T(8,128)(2,1)S(1)} %collective-permute-done.4), channel_id=1, source_target_pairs={{0,1},{1,2},{2,3},{3,4},{4,5},{5,6},{6,7},{7,0},{8,9},{9,10},{10,1... | collective-permute-start | bytes 1572872 | tf_op jit(solution)/shard_map/ppermute | solution.py:19
  175.1 1.1 copy-start.19
  175.4 13.4 %copy-start.15 = (bf16[384,128]{1,0:T(8,128)(2,1)S(1)}, bf16[384,128]{1,0:T(8,128)(2,1)}, u32[]{:S(2)}) copy-start(bf16[384,128]{1,0:T(8,128)(2,1)} %param.31) | copy-start | bytes 294916
  176.2 18.7 %copy-start.12 = (bf16[128,688]{0,1:T(8,128)(2,1)S(1)}, bf16[128,688]{0,1:T(8,128)(2,1)}, u32[]{:S(2)}) copy-start(bf16[128,688]{0,1:T(8,128)(2,1)} %param.34) | copy-start | bytes 528388
  176.2 18.7 %copy-start.13 = (bf16[128,688]{0,1:T(8,128)(2,1)S(1)}, bf16[128,688]{0,1:T(8,128)(2,1)}, u32[]{:S(2)}) copy-start(bf16[128,688]{0,1:T(8,128)(2,1)} %param.33) | copy-start | bytes 528388
  176.4 2.1 copy-start.6
  178.5 18.0 %copy-start.23 = (f32[384]{0:T(512)S(1)}, f32[384]{0:T(512)}, u32[]{:S(2)}) copy-start(f32[384]{0:T(512)} %param.29) | copy-start | bytes 4612
  178.5 7.9 %collective-permute-start.7 = (bf16[128,2048]{1,0:T(8,128)(2,1)S(1)}, bf16[128,2048]{1,0:T(8,128)(2,1)S(1)}, u32[]{:S(2)}, u32[]{:S(2)}) collective-permute-start(bf16[128,2048]{1,0:T(8,128)(2,1)S(1)} %get-tuple-element.10), channel_id=1, source_target_pairs={{0,1},{1,2},{2,3},{3,4},{4,5},{5,6},{6,7},{7,0},{8,9},{9,10},{10,1... | collective-permute-start | bytes 1572872 | tf_op jit(solution)/shard_map/ppermute | solution.py:19
  180.2 15.5 %collective-permute-start.8 = (bf16[128,2048]{1,0:T(8,128)(2,1)S(1)}, bf16[128,2048]{1,0:T(8,128)(2,1)S(1)}, u32[]{:S(2)}, u32[]{:S(2)}) collective-permute-start(bf16[128,2048]{1,0:T(8,128)(2,1)S(1)} %get-tuple-element.10), channel_id=1, source_target_pairs={{0,7},{1,0},{2,1},{3,2},{4,3},{5,4},{6,5},{7,6},{8,15},{9,8},{10,9... | collective-permute-start | bytes 1572872 | tf_op jit(solution)/shard_map/ppermute | solution.py:24
  186.4 10.1 %collective-permute-start.9 = (bf16[128,2048]{1,0:T(8,128)(2,1)S(1)}, bf16[128,2048]{1,0:T(8,128)(2,1)S(1)}, u32[]{:S(2)}, u32[]{:S(2)}) collective-permute-start(bf16[128,2048]{1,0:T(8,128)(2,1)S(1)} %collective-permute-done.7), channel_id=1, source_target_pairs={{0,1},{1,2},{2,3},{3,4},{4,5},{5,6},{6,7},{7,0},{8,9},{9,10},{10,1... | collective-permute-start | bytes 1572872 | tf_op jit(solution)/shard_map/ppermute | solution.py:19
  190.3 173.0 %all-to-all-start.2 = ((bf16[16,384,128]{1,2,0:T(8,128)(2,1)}), bf16[16,384,128]{1,2,0:T(8,128)(2,1)}, u32[]{:S(2)}, u32[]{:S(2)}) async-start(bf16[16,384,128]{1,2,0:T(8,128)(2,1)} %broadcast_in_dim.26), calls=%async_computation.2 | async-start | bytes 3145728 | tf_op jit(solution)/shard_map/all_to_all | solution.py:42
  194.7 280.7 %all-gather.8.cloned.1.call-start = ((), (), s32[]{:S(2)}) async-start(), calls=%async_computation.8 | async-start | bytes 5988352 | tf_op jit(solution)/shard_map/all_gather | solution.py:33
  195.8 9.0 %collective-permute-start.10 = (bf16[128,2048]{1,0:T(8,128)(2,1)S(1)}, bf16[128,2048]{1,0:T(8,128)(2,1)S(1)}, u32[]{:S(2)}, u32[]{:S(2)}) collective-permute-start(bf16[128,2048]{1,0:T(8,128)(2,1)S(1)} %collective-permute-done.8), channel_id=1, source_target_pairs={{0,7},{1,0},{2,1},{3,2},{4,3},{5,4},{6,5},{7,6},{8,15},{9,8},{10,9... | collective-permute-start | bytes 1572872 | tf_op jit(solution)/shard_map/ppermute | solution.py:24
  196.5 10.3 %collective-permute-start.11 = (bf16[128,2048]{1,0:T(8,128)(2,1)S(1)}, bf16[128,2048]{1,0:T(8,128)(2,1)S(1)}, u32[]{:S(2)}, u32[]{:S(2)}) collective-permute-start(bf16[128,2048]{1,0:T(8,128)(2,1)S(1)} %collective-permute-done.9), channel_id=1, source_target_pairs={{0,1},{1,2},{2,3},{3,4},{4,5},{5,6},{6,7},{7,0},{8,9},{9,10},{10,1... | collective-permute-start | bytes 1572872 | tf_op jit(solution)/shard_map/ppermute | solution.py:19
  204.8 9.0 %collective-permute-start.12 = (bf16[128,2048]{1,0:T(8,128)(2,1)S(1)}, bf16[128,2048]{1,0:T(8,128)(2,1)S(1)}, u32[]{:S(2)}, u32[]{:S(2)}) collective-permute-start(bf16[128,2048]{1,0:T(8,128)(2,1)S(1)} %collective-permute-done.10), channel_id=1, source_target_pairs={{0,7},{1,0},{2,1},{3,2},{4,3},{5,4},{6,5},{7,6},{8,15},{9,8},{10,9... | collective-permute-start | bytes 1572872 | tf_op jit(solution)/shard_map/ppermute | solution.py:24
  206.8 7.9 %collective-permute-start.13 = (bf16[128,2048]{1,0:T(8,128)(2,1)S(1)}, bf16[128,2048]{1,0:T(8,128)(2,1)S(1)}, u32[]{:S(2)}, u32[]{:S(2)}) collective-permute-start(bf16[128,2048]{1,0:T(8,128)(2,1)S(1)} %collective-permute-done.11), channel_id=1, source_target_pairs={{0,1},{1,2},{2,3},{3,4},{4,5},{5,6},{6,7},{7,0},{8,9},{9,10},{10,1... | collective-permute-start | bytes 1572872 | tf_op jit(solution)/shard_map/ppermute | solution.py:19
  224.4 1.7 copy-start.24
  226.7 1.6 copy-start.22
  338.9 16.6 %copy-start.16 = (f32[16,384]{1,0:T(8,128)S(1)}, f32[16,384]{1,0:T(8,128)}, u32[]{:S(2)}) copy-start(f32[16,384]{1,0:T(8,128)} %pad_maximum_fusion.8) | copy-start | bytes 73732
  338.9 16.6 %copy-start.17 = (f32[16,384]{1,0:T(8,128)S(1)}, f32[16,384]{1,0:T(8,128)}, u32[]{:S(2)}) copy-start(f32[16,384]{1,0:T(8,128)} %add.341) | copy-start | bytes 73732
  352.7 5.1 copy-start.10
  355.6 2.4 copy-start.8
  355.6 2.4 copy-start.9
  358.5 3.3 copy-start.7
  432.6 2.9 copy-start.20
  432.9 14.4 %copy-start.14 = (bf16[688,128]{1,0:T(8,128)(2,1)S(1)}, bf16[688,128]{1,0:T(8,128)(2,1)}, u32[]{:S(2)}) copy-start(bf16[688,128]{1,0:T(8,128)(2,1)} %param.35) | copy-start | bytes 528388
  436.6 8.2 %collective-permute-start.14 = (bf16[128,2048]{1,0:T(8,128)(2,1)}, bf16[128,2048]{1,0:T(8,128)(2,1)}, u32[]{:S(2)}, u32[]{:S(2)}) collective-permute-start(bf16[128,2048]{1,0:T(8,128)(2,1)} %get-tuple-element.6), channel_id=1, source_target_pairs={{0,1},{1,2},{2,3},{3,4},{4,5},{5,6},{6,7},{7,0},{8,9},{9,10},{10,1... | collective-permute-start | bytes 1572872 | tf_op jit(solution)/shard_map/ppermute | solution.py:19
  438.4 17.3 %collective-permute-start.15 = (bf16[128,2048]{1,0:T(8,128)(2,1)}, bf16[128,2048]{1,0:T(8,128)(2,1)}, u32[]{:S(2)}, u32[]{:S(2)}) collective-permute-start(bf16[128,2048]{1,0:T(8,128)(2,1)} %get-tuple-element.6), channel_id=1, source_target_pairs={{0,7},{1,0},{2,1},{3,2},{4,3},{5,4},{6,5},{7,6},{8,15},{9,8},{10,9... | collective-permute-start | bytes 1572872 | tf_op jit(solution)/shard_map/ppermute | solution.py:24
  444.8 11.7 %collective-permute-start.16 = (bf16[128,2048]{1,0:T(8,128)(2,1)}, bf16[128,2048]{1,0:T(8,128)(2,1)}, u32[]{:S(2)}, u32[]{:S(2)}) collective-permute-start(bf16[128,2048]{1,0:T(8,128)(2,1)} %collective-permute-done.14), channel_id=1, source_target_pairs={{0,1},{1,2},{2,3},{3,4},{4,5},{5,6},{6,7},{7,0},{8,9},{9,10},{10,1... | collective-permute-start | bytes 1572872 | tf_op jit(solution)/shard_map/ppermute | solution.py:19
  449.3 48.7 %all-to-all-start.4 = ((bf16[16,688,128]{2,1,0:T(8,128)(2,1)}), bf16[16,688,128]{2,1,0:T(8,128)(2,1)S(1)}, u32[]{:S(2)}, u32[]{:S(2)}) async-start(bf16[16,688,128]{2,1,0:T(8,128)(2,1)} %broadcast_in_dim.27), calls=%async_computation.4 | async-start | bytes 5636096 | tf_op jit(solution)/shard_map/all_to_all | solution.py:42
  455.7 9.1 %collective-permute-start.17 = (bf16[128,2048]{1,0:T(8,128)(2,1)}, bf16[128,2048]{1,0:T(8,128)(2,1)S(1)}, u32[]{:S(2)}, u32[]{:S(2)}) collective-permute-start(bf16[128,2048]{1,0:T(8,128)(2,1)} %collective-permute-done.15), channel_id=1, source_target_pairs={{0,7},{1,0},{2,1},{3,2},{4,3},{5,4},{6,5},{7,6},{8,15},{9,8},{10,9... | collective-permute-start | bytes 1572872 | tf_op jit(solution)/shard_map/ppermute | solution.py:24
  456.5 11.6 %collective-permute-start.18 = (bf16[128,2048]{1,0:T(8,128)(2,1)}, bf16[128,2048]{1,0:T(8,128)(2,1)S(1)}, u32[]{:S(2)}, u32[]{:S(2)}) collective-permute-start(bf16[128,2048]{1,0:T(8,128)(2,1)} %collective-permute-done.16), channel_id=1, source_target_pairs={{0,1},{1,2},{2,3},{3,4},{4,5},{5,6},{6,7},{7,0},{8,9},{9,10},{10,1... | collective-permute-start | bytes 1572872 | tf_op jit(solution)/shard_map/ppermute | solution.py:19
  464.8 8.9 %collective-permute-start.19 = (bf16[128,2048]{1,0:T(8,128)(2,1)S(1)}, bf16[128,2048]{1,0:T(8,128)(2,1)S(1)}, u32[]{:S(2)}, u32[]{:S(2)}) collective-permute-start(bf16[128,2048]{1,0:T(8,128)(2,1)S(1)} %collective-permute-done.17), channel_id=1, source_target_pairs={{0,7},{1,0},{2,1},{3,2},{4,3},{5,4},{6,5},{7,6},{8,15},{9,8},{10,9... | collective-permute-start | bytes 1572872 | tf_op jit(solution)/shard_map/ppermute | solution.py:24
  468.1 6.5 %collective-permute-start.20 = (bf16[128,2048]{1,0:T(8,128)(2,1)S(1)}, bf16[128,2048]{1,0:T(8,128)(2,1)S(1)}, u32[]{:S(2)}, u32[]{:S(2)}) collective-permute-start(bf16[128,2048]{1,0:T(8,128)(2,1)S(1)} %collective-permute-done.18), channel_id=1, source_target_pairs={{0,1},{1,2},{2,3},{3,4},{4,5},{5,6},{6,7},{7,0},{8,9},{9,10},{10,1... | collective-permute-start | bytes 1572872 | tf_op jit(solution)/shard_map/ppermute | solution.py:19
  509.2 55.6 %copy-start.1 = (bf16[2,192,192]{2,1,0:T(8,128)(2,1)S(1)}, bf16[2,192,192]{2,1,0:T(8,128)(2,1)}, u32[]{:S(2)}) copy-start(bf16[2,192,192]{2,1,0:T(8,128)(2,1)} %param.27) | copy-start | bytes 442372
  (6 other events, 5.0 us)
Sparse Core Ops, SparseCore 0:
  9.4 90.7 all-gather.3
  102.4 47.7 all-gather.5
  197.7 66.1 all-gather.7
